TPU v7x, 32 devices: a whole 2x2x4 slice. The times are simulated.
32 devices in a mesh: sp: 8 (over z, y), tp: 4 (over x, core).
Axes of the slice: x: 2, y: 2, z: 4, core: 2. Of those that a mesh axis runs over, the one named last changes fastest.
Arguments:
- stream_in: bfloat16 [4096, 4096], P('sp', 'tp'), may hold values from -12 to 12
- norm_gain: float32 [2, 4096], replicated, may hold values from 0.1 to 1.9
- value_proj: bfloat16 [2, 4096, 4096], P(None, 'sp', 'tp'), may hold values from -0.09375 to 0.09375
- gate_proj: bfloat16 [2, 4096, 4096], P(None, 'sp', 'tp'), may hold values from -0.09375 to 0.09375
- out_proj: bfloat16 [2, 4096, 4096], P(None, 'sp', 'tp'), may hold values from -0.1875 to 0.1875
- conv_taps: float32 [2, 4, 4096], replicated, may hold values from -3 to 3
- block_gates: bfloat16 [2, 2, 2, 4096, 128], P(None, None, None, 'tp'), may hold values from -0.5 to 0.5
- forget_rate: float32 [2, 2, 4096], replicated, may hold values from 0 to 0.05, as said below
Outputs:
- stream_out: bfloat16 [4096, 4096], P('sp', 'tp')
Inputs may be any that keep to these rules, and one draw needn't show every extreme that they name: `forget_rate`: positive.
All inputs are finite; a program needn't handle non-finite values.
Results may differ from a plain program's by a relative error of at most 0.025.
Values may be sent and summed in bfloat16 or wider, within the bound.
A program may use at most 192 MiB of HBM per device.

v0:
```python
import functools

import jax
import jax.numpy as jnp
from jax import lax
from jax.experimental import pallas as pl
from jax.experimental.pallas import tpu as pltpu
from jax.sharding import PartitionSpec as P

GATE_SCALE = 8.0
NORM_EPS = 1e-06
ROW_STEPS = 4
CHUNKS = 8
MESH = pl.DeviceIdType.MESH
VMEM_BYTES = 67043328
SERIES = (1.0, -1.0 / 2, 1.0 / 6, -1.0 / 24, 1.0 / 120, -1.0 / 720, 1.0 / 5040)


def rem(a, b):
    return lax.rem(a, jnp.int32(b))


def div(a, b):
    return lax.div(a, jnp.int32(b))


def flip_bits(a, b, count):
    total, bit = 0, 1
    while bit < count:
        total = total + bit * rem(div(a, bit) + (b // bit if isinstance(b, int) else div(b, bit)), 2)
        bit *= 2
    return total


def role_of(z):
    return rem(z + div(z, 2), 2)


def sigmoid(x):
    return 0.5 * jnp.tanh(0.5 * x) + 0.5


def kernel(
    nsp, ntp, layers,
    stream_ref, value_ref, gate_ref, back_ref, gain_ref, taps_hbm, gates_hbm, rate_hbm,
    result_ref,
    feats, weights, own, mix, gate_z, padded, fa, fu, ba, bu, fh, fp, bh, bp,
    both, fcum, bcum, mixed, part, core_in, x_in, z_in, edges, ends, states, taps, gates, rate,
    start_sem, own_sem, wz_send, wy_send, w_recv,
    fz_send, fz_recv, fx_send, fx_recv, fc_send, fc_recv,
    sz_send, sz_recv, sx_send, sx_recv, sc_send, sc_recv,
    edge_send, edge_recv, end_send, end_recv, out_sem,
):
    ny = 1 << ((nsp.bit_length() - 1) // 2)
    nz, nx, groups, per = nsp // ny, ntp // 2, nsp // 2, nsp // ntp
    rank, column = lax.axis_index("sp"), lax.axis_index("tp")
    z, y, x, core = div(rank, ny), rem(rank, ny), div(column, 2), rem(column, 2)
    role = role_of(z)
    group = div(z, 2) * ny + y
    rows, width = mix.shape[1], mix.shape[2]
    depth = weights.shape[2]
    block = gates.shape[3]
    sources = (value_ref, gate_ref, back_ref)

    def z_peer(k):
        return (flip_bits(z, k, nz) * ny + y, column)

    def y_peer(k):
        return (z * ny + rem(y + k, ny), column)

    def x_peer(k):
        return (rank, rem(x + k, nx) * 2 + core)

    def group_peer(k):
        g = rem(group + k, groups)
        half = div(g, ny)
        return ((2 * half + rem(role + half, 2)) * ny + rem(g, ny), column)

    core_peer = (rank, x * 2 + 1 - core)
    peers = [z_peer(k) for k in range(1, nz)] + [y_peer(k) for k in range(1, ny)]
    peers += [x_peer(k) for k in range(1, nx)] + [core_peer]
    peers += [group_peer(k) for k in range(1, groups)]
    barrier = pltpu.get_barrier_semaphore()
    for peer in peers:
        pl.semaphore_signal(barrier, inc=1, device_id=peer, device_id_type=MESH)

    def remote(src, dst, send, recv, peer):
        return pltpu.make_async_remote_copy(
            src_ref=src, dst_ref=dst, send_sem=send, recv_sem=recv,
            device_id=peer, device_id_type=MESH,
        )

    def rows_of(m, which):
        return sources[m % 3].at[m // 3, :, pl.ds(pl.multiple_of(which * width, 128), width)]

    def own_weight(m):
        return pltpu.make_async_copy(rows_of(m, role), weights.at[m, 0], own_sem.at[m])

    def z_weight(m, k):
        there = role_of(flip_bits(z, k, nz))
        return remote(
            rows_of(m, there), weights.at[m, k * ny], wz_send.at[m, k - 1],
            w_recv.at[m, k * ny], z_peer(k),
        )

    def y_weight(m, kz, ky, first=False):
        src = rows_of(m, role) if first else weights.at[m, kz * ny]
        return remote(
            src, weights.at[m, kz * ny + ky], wy_send.at[m, kz, ky - 1],
            w_recv.at[m, kz * ny + ky], y_peer(ky),
        )

    def send_weights(ms):
        for k in range(1, nz):
            for m in ms:
                z_weight(m, k).start()

    def send_own_weights(ms):
        for m in ms:
            for ky in range(1, ny):
                y_weight(m, 0, ky, True).start()

    def relay(m, kz):
        z_weight_wait(m, kz)
        for ky in range(1, ny):
            y_weight(m, kz, ky).start()

    def z_weight_wait(m, kz):
        remote(
            weights.at[m, kz * ny], weights.at[m, kz * ny], wz_send.at[m, 0],
            w_recv.at[m, kz * ny], core_peer,
        ).wait_recv()

    def y_weight_wait(m, p):
        remote(
            weights.at[m, p], weights.at[m, p], wz_send.at[m, 0], w_recv.at[m, p], core_peer
        ).wait_recv()

    def f_copy(src, slot, at_column, send, recv, peer):
        return remote(src, feats.at[slot, at_column], send, recv, peer)

    def column_of(k):
        return rem(x + nx - k, nx) * 2 + core

    def f_to_core(slot, k, src):
        return f_copy(
            src, slot, column_of(k), fc_send.at[slot, k], fc_recv.at[slot, k], core_peer
        )

    def f_to_x(slot, k, src):
        return f_copy(
            src, slot, column, fx_send.at[slot, k - 1], fx_recv.at[slot, k - 1], x_peer(k)
        )

    def gather_start(src):
        z_copy = f_copy(src, 1, column, fz_send.at[0], fz_recv.at[0], z_peer(1))
        z_copy.start()
        for k in range(1, nx):
            f_to_x(0, k, src).start()
        f_to_core(0, 0, src).start()

    def gather_rest():
        f_copy(own, 1, column, fz_send.at[0], fz_recv.at[0], z_peer(1)).wait_recv()
        mine = feats.at[1, column]
        for k in range(1, nx):
            f_to_x(1, k, mine).start()
        f_to_core(1, 0, mine).start()
        for slot in range(2):
            for k in range(1, nx):
                there = feats.at[slot, column_of(k)]
                remote(
                    own, there, fx_send.at[slot, k - 1], fx_recv.at[slot, k - 1], core_peer
                ).wait_recv()
                f_to_core(slot, k, there).start()

    def gather_finish(slot):
        for k in range(nx):
            there = feats.at[slot, column_of(k)]
            f_to_core(slot, k, there).wait_recv()
            f_to_core(slot, k, there).wait_send()
        for k in range(1, nx):
            f_to_x(slot, k, own).wait_send()
        if slot == 1:
            f_copy(own, 1, column, fz_send.at[0], fz_recv.at[0], z_peer(1)).wait_send()

    def normalize(layer, slot):
        step = 16

        def body(i, _):
            at = pl.ds(pl.multiple_of(i * step, step), step)
            squares = None
            for t in range(ntp):
                values = feats[slot, t, at, :].astype(jnp.float32)
                total = jnp.sum(values * values, axis=1, keepdims=True)
                squares = total if squares is None else squares + total
            size = feats.shape[3]
            scale = lax.rsqrt(squares / (ntp * size) + NORM_EPS)
            for t in range(ntp):
                values = feats[slot, t, at, :].astype(jnp.float32)
                gain = gain_ref[layer : layer + 1, t * size : (t + 1) * size]
                feats[slot, t, at, :] = (values * scale * gain).astype(jnp.bfloat16)
            return 0

        lax.fori_loop(0, rows // step, body, 0)

    def owner_of(p):
        kz, ky = div(p, ny), rem(p, ny)
        return flip_bits(z, kz, nz) * ny + rem(y + ny - ky, ny)

    def enter(layer, relayed):
        fcum[...] = jnp.zeros_like(fcum)
        bcum[...] = jnp.zeros_like(bcum)
        first, second = 3 * layer, 3 * layer + 1

        def body(p, _):
            ky = rem(p, ny)
            for m in (first, second):

                @pl.when(ky != 0)
                def _():
                    y_weight_wait(m, p)

                if m not in relayed:

                    @pl.when(jnp.logical_and(ky == 0, p != 0))
                    def _():
                        relay(m, div(p, ny))

            owner = owner_of(p)
            t = div(owner, per)
            at = pl.ds(pl.multiple_of(rem(owner, per) * depth, 128), depth)
            for slot in range(2):
                cells = feats[slot, t, :, at]
                for m, total in ((first, fcum), (second, bcum)):
                    total[slot] += jnp.dot(
                        cells, weights[m, p], preferred_element_type=jnp.float32
                    )
            return 0

        for m in (first, second):
            own_weight(m).wait()
        lax.fori_loop(0, nsp, body, 0)
        for slot in range(2):
            mix[slot] = fcum[slot].astype(jnp.bfloat16)
            gate_z[slot] = bcum[slot].astype(jnp.bfloat16)

    def parity(slot):
        return rem(z + slot, 2)

    def token_block(slot):
        return flip_bits(z, slot, nz) * ny + y

    def place_of(b):
        zb, yb = div(b, ny), rem(b, ny)
        there = div(zb, 2) * ny + yb
        return rem(group + groups - there, groups), rem(zb, 2)

    def exchange(cells, send, recv):
        copies = [
            remote(cells.at[0], cells.at[k], send.at[k - 1], recv.at[k - 1], group_peer(k))
            for k in range(1, groups)
        ]
        for copy in copies:
            copy.start()
        for copy in copies:
            copy.wait_recv()
        for copy in copies:
            copy.wait_send()

    def exchange_edges():
        ends[0] = jnp.zeros(ends.shape[1:], jnp.float32)
        for slot in range(2):
            edges[0, parity(slot), 0:8, :] = mix[slot, rows - 8 : rows, :].astype(jnp.float32)
            edges[0, parity(slot), 8:16, :] = mix[slot, 0:8, :].astype(jnp.float32)
        exchange(edges, edge_send, edge_recv)

    def scan(layer, services):
        blocks = width // block
        chunk = rows // CHUNKS
        size = rows // ROW_STEPS

        def body(i, _):
            for when, m, kz in services:

                @pl.when(i == when)
                def _():
                    relay(m, kz)

            slot, b = div(i, blocks), rem(i, blocks)
            lanes = pl.ds(pl.multiple_of(b * block, 128), block)
            where = flip_bits(z, slot, nz) * ny + y
            even = rem(z + slot, 2)
            off, par = place_of(jnp.maximum(where - 1, 0))
            padded[0:8, :] = jnp.where(where > 0, edges[off, par, 0:8, lanes], 0.0)
            off, par = place_of(jnp.minimum(where + 1, nsp - 1))
            padded[rows + 8 : rows + 16, :] = jnp.where(
                where < nsp - 1, edges[off, par, 8:16, lanes], 0.0
            )
            padded[8 : rows + 8, :] = mix[slot, :, lanes].astype(jnp.float32)
            maps = jnp.concatenate([gates[layer, g, lanes, :] for g in range(4)], axis=1)
            maps = jnp.concatenate([maps, maps], axis=0)
            for step in range(ROW_STEPS):
                base = step * size
                conv = padded[base + 6 : base + 6 + size, :] * taps[layer, 0:1, lanes]
                for tap in range(1, 4):
                    conv += (
                        padded[base + 6 + tap : base + 6 + tap + size, :]
                        * taps[layer, tap : tap + 1, lanes]
                    )
                high = conv.astype(jnp.bfloat16)
                low = (conv - high.astype(jnp.float32)).astype(jnp.bfloat16)
                pre = jnp.dot(
                    jnp.concatenate([high, low], axis=1), maps, preferred_element_type=jnp.float32
                )
                for e, (decay_to, drive_to) in enumerate(((fa, fu), (ba, bu))):
                    pre_r = pre[:, 2 * e * block : (2 * e + 1) * block]
                    pre_i = pre[:, (2 * e + 1) * block : (2 * e + 2) * block]
                    speed = GATE_SCALE * rate[layer, e : e + 1, lanes]
                    fall = sigmoid(pre_r) * speed
                    series = jnp.full_like(fall, SERIES[-1])
                    for term in reversed(SERIES[:-1]):
                        series = series * fall + term
                    lost = fall * series
                    loss = lost * (2.0 - lost)
                    root = loss * lax.rsqrt(jnp.maximum(loss, 1e-30))
                    decay_to[base : base + size, :] = 1.0 - lost
                    drive_to[base : base + size, :] = root * sigmoid(pre_i) * conv

            def advance(j, carry):
                f_state, f_prod, b_state, b_prod = carry
                at = pl.ds(j, CHUNKS, stride=chunk)
                back = pl.ds(chunk - 1 - j, CHUNKS, stride=chunk)
                f_decay, b_decay = fa[at, :], ba[back, :]
                f_state = f_decay * f_state + fu[at, :]
                f_prod = f_decay * f_prod
                b_state = b_decay * b_state + bu[back, :]
                b_prod = b_decay * b_prod
                fh[at, :] = f_state
                fp[at, :] = f_prod
                bh[back, :] = b_state
                bp[back, :] = b_prod
                return f_state, f_prod, b_state, b_prod

            zeros = jnp.zeros((CHUNKS, block), jnp.float32)
            ones = jnp.ones((CHUNKS, block), jnp.float32)
            f_state, f_prod, b_state, b_prod = lax.fori_loop(
                0, chunk, advance, (zeros, ones, zeros, ones), unroll=8
            )
            f_in, b_in = [], [None] * CHUNKS
            state, prod = zeros[0:1], ones[0:1]
            for c in range(CHUNKS):
                f_in.append((state, prod))
                state = f_prod[c : c + 1] * state + f_state[c : c + 1]
                prod = f_prod[c : c + 1] * prod
            ends[0, even, 0:1, lanes] = prod
            ends[0, even, 1:2, lanes] = state
            state, prod = zeros[0:1], ones[0:1]
            for c in reversed(range(CHUNKS)):
                b_in[c] = (state, prod)
                state = b_prod[c : c + 1] * state + b_state[c : c + 1]
                prod = b_prod[c : c + 1] * prod
            ends[0, even, 2:3, lanes] = prod
            ends[0, even, 3:4, lanes] = state
            for c in range(CHUNKS):
                at = slice(c * chunk, (c + 1) * chunk)
                f_local, b_local = fp[at, :], bp[at, :]
                both[slot, at, lanes] = (
                    fh[at, :] + f_local * f_in[c][0] + bh[at, :] + b_local * b_in[c][0]
                )
                fcum[slot, at, lanes] = f_local * f_in[c][1]
                bcum[slot, at, lanes] = b_local * b_in[c][1]
            return 0

        lax.fori_loop(0, 2 * blocks, body, 0)

    def exchange_ends():
        exchange(ends, end_send, end_recv)
        for slot in range(2):
            where = token_block(slot)
            forward = jnp.zeros((1, width), jnp.float32)
            backward = jnp.zeros((1, width), jnp.float32)
            for b in range(nsp - 1):
                off, par = place_of(jnp.int32(b))
                moved = ends[off, par, 0:1, :] * forward + ends[off, par, 1:2, :]
                forward = jnp.where(where > b, moved, forward)
            for b in range(nsp - 1, 0, -1):
                off, par = place_of(jnp.int32(b))
                moved = ends[off, par, 2:3, :] * backward + ends[off, par, 3:4, :]
                backward = jnp.where(where < b, moved, backward)
            states[slot, 0:1, :] = forward
            states[slot, 1:2, :] = backward

    def leave(layer, slot, first):
        step = 32
        m = 3 * layer + 2

        def finish(i, _):
            at = pl.ds(pl.multiple_of(i * step, step), step)
            total = both[slot, at, :] + fcum[slot, at, :] * states[slot, 0:1, :]
            total = total + bcum[slot, at, :] * states[slot, 1:2, :]
            gate = gate_z[slot, at, :].astype(jnp.float32)
            mixed[at, :] = (total * gate * sigmoid(gate)).astype(jnp.bfloat16)
            return 0

        lax.fori_loop(0, rows // step, finish, 0)

        def body(p, _):
            if first:

                @pl.when(rem(p, ny) != 0)
                def _():
                    y_weight_wait(m, p)

            term = lax.dot_general(
                mixed[...], weights[m, p], (((1,), (1,)), ((), ())),
                preferred_element_type=jnp.float32,
            )
            owner = owner_of(p)
            t = div(owner, per)
            far = rem(div(t, 2) + nx - x, nx)
            other = rem(t + core, 2)
            at = pl.ds(pl.multiple_of(rem(owner, per) * depth, 128), depth)
            part[slot, other, far, :, at] = term.astype(jnp.bfloat16)
            return 0

        if first:
            own_weight(m).wait()
        lax.fori_loop(0, nsp, body, 0)

    def s_to_core(slot, k):
        return remote(
            part.at[slot, 1, k], core_in.at[slot, k], sc_send.at[slot, k], sc_recv.at[slot, k],
            core_peer,
        )

    def s_to_x(slot, k):
        return remote(
            part.at[slot, 0, k], x_in.at[slot, k - 1], sx_send.at[slot, k - 1],
            sx_recv.at[slot, k - 1], x_peer(k),
        )

    def s_to_z():
        return remote(part.at[1, 0, 0], z_in, sz_send.at[0], sz_recv.at[0], z_peer(1))

    def give(slot):
        for k in list(range(1, nx)) + [0]:
            s_to_core(slot, k).start()

    def tiles(body):
        step = 32

        def run(i, _):
            body(pl.ds(pl.multiple_of(i * step, step), step))
            return 0

        lax.fori_loop(0, rows // step, run, 0)

    def pass_on(slot):
        for k in range(1, nx):
            s_to_core(slot, k).wait_recv()

            def body(at):
                total = part[slot, 0, k, at, :].astype(jnp.float32)
                total = total + core_in[slot, k, at, :].astype(jnp.float32)
                part[slot, 0, k, at, :] = total.astype(jnp.bfloat16)

            tiles(body)
            s_to_x(slot, k).start()
        s_to_core(slot, 0).wait_recv()

    def summed(slot, at):
        total = part[slot, 0, 0, at, :].astype(jnp.float32)
        total = total + core_in[slot, 0, at, :].astype(jnp.float32)
        for k in range(1, nx):
            total = total + x_in[slot, k - 1, at, :].astype(jnp.float32)
        return total

    def land(slot):
        for k in range(1, nx):
            s_to_x(slot, k).wait_recv()

    def drain(slot):
        for k in range(nx):
            s_to_core(slot, k).wait_send()
        for k in range(1, nx):
            s_to_x(slot, k).wait_send()

    first_own = pltpu.make_async_copy(stream_ref, own, start_sem.at[0])
    first_feat = pltpu.make_async_copy(stream_ref, feats.at[0, column], start_sem.at[1])
    channel = pl.multiple_of(column * 2 * width + role * width, 128)
    small = [
        pltpu.make_async_copy(taps_hbm.at[:, :, pl.ds(channel, width)], taps, start_sem.at[2]),
        pltpu.make_async_copy(rate_hbm.at[:, :, pl.ds(channel, width)], rate, start_sem.at[3]),
        pltpu.make_async_copy(
            gates_hbm.at[:, :, pl.ds(pl.multiple_of(role * width, 128), width), :],
            gates, start_sem.at[4],
        ),
    ]
    first_own.start()
    first_feat.start()
    pl.semaphore_wait(barrier, len(peers))
    gather_start(stream_ref)
    send_weights((0, 1))
    send_own_weights((0, 1))
    for m in range(3 * layers):
        own_weight(m).start()
    for copy in small:
        copy.start()
    send_weights((2,))
    send_own_weights((2,))

    for layer in range(layers):
        last = layer == layers - 1
        gather_rest()
        if layer == 0:
            first_own.wait()
            first_feat.wait()
        for slot in range(2):
            gather_finish(slot)
            normalize(layer, slot)
        enter(layer, () if layer == 0 else (3 * layer,))
        exchange_edges()
        if not last:
            send_weights((3 * layer + 3,))
            send_own_weights((3 * layer + 3,))
        if layer == 0:
            for copy in small:
                copy.wait()
        blocks = 2 * (width // block)
        services = [
            (min(blocks - 1, (blocks * (k + 1)) // (nz + 1)), 3 * layer + 2, k)
            for k in range(1, nz)
        ]
        scan(layer, services)
        exchange_ends()
        leave(layer, 1, True)
        give(1)
        leave(layer, 0, False)
        pass_on(1)
        give(0)
        pass_on(0)
        if not last:
            for k in range(1, nz):
                relay(3 * layer + 3, k)
        land(1)

        def send_over(at):
            part[1, 0, 0, at, :] = summed(1, at).astype(jnp.bfloat16)

        tiles(send_over)
        s_to_z().start()
        land(0)
        s_to_z().wait_recv()

        def renew(at):
            total = summed(0, at) + z_in[at, :].astype(jnp.float32)
            fresh = (own[at, :].astype(jnp.float32) + total).astype(jnp.bfloat16)
            own[at, :] = fresh
            if not last:
                feats[0, column, at, :] = fresh

        tiles(renew)
        if not last:
            gather_start(own)
            send_weights((3 * layer + 4, 3 * layer + 5))
            send_own_weights((3 * layer + 4, 3 * layer + 5))
        drain(1)
        drain(0)
        s_to_z().wait_send()
    result = pltpu.make_async_copy(own, result_ref, out_sem.at[0])
    result.start()
    for m in range(3 * layers):
        for k in range(1, nz):
            z_weight(m, k).wait_send()
        for kz in range(nz):
            for ky in range(1, ny):
                y_weight(m, kz, ky, kz == 0).wait_send()
    result.wait()


def per_device(
    stream_in, norm_gain, value_proj, gate_proj, out_proj, conv_taps, block_gates, forget_rate
):
    nsp, ntp = lax.axis_size("sp"), lax.axis_size("tp")
    layers, depth, both_roles = value_proj.shape
    rows, size = stream_in.shape
    width = both_roles // 2
    block = block_gates.shape[-1]
    ny = 1 << ((nsp.bit_length() - 1) // 2)
    nz, nx, groups = nsp // ny, ntp // 2, nsp // 2
    maps = block_gates.reshape(layers, 4, both_roles, block)
    half, full = jnp.bfloat16, jnp.float32
    dma = pltpu.SemaphoreType.DMA
    slab = pltpu.VMEM((rows, block), full)
    scratch = [
        pltpu.VMEM((2, ntp, rows, size), half),
        pltpu.VMEM((3 * layers, nsp, depth, width), half),
        pltpu.VMEM((rows, size), half),
        pltpu.VMEM((2, rows, width), half),
        pltpu.VMEM((2, rows, width), half),
        pltpu.VMEM((rows + 16, block), full),
        *[slab] * 8,
        *[pltpu.VMEM((2, rows, width), full)] * 3,
        pltpu.VMEM((rows, width), half),
        pltpu.VMEM((2, 2, nx, rows, size), half),
        pltpu.VMEM((2, nx, rows, size), half),
        pltpu.VMEM((2, nx - 1, rows, size), half),
        pltpu.VMEM((rows, size), half),
        pltpu.VMEM((groups, 2, 16, width), full),
        pltpu.VMEM((groups, 2, 8, width), full),
        pltpu.VMEM((2, 8, width), full),
        pltpu.VMEM((layers, 4, width), full),
        pltpu.VMEM((layers, 4, width, block), half),
        pltpu.VMEM((layers, 2, width), full),
        dma((5,)),
        dma((3 * layers,)),
        dma((3 * layers, nz - 1)),
        dma((3 * layers, nz, ny - 1)),
        dma((3 * layers, nsp)),
        dma((1,)), dma((1,)), dma((2, nx - 1)), dma((2, nx - 1)), dma((2, nx)), dma((2, nx)),
        dma((1,)), dma((1,)), dma((2, nx - 1)), dma((2, nx - 1)), dma((2, nx)), dma((2, nx)),
        dma((groups - 1,)), dma((groups - 1,)), dma((groups - 1,)), dma((groups - 1,)),
        dma((1,)),
    ]
    anywhere = pl.BlockSpec(memory_space=pl.ANY)
    inside = pl.BlockSpec(memory_space=pltpu.VMEM)
    return pl.pallas_call(
        functools.partial(kernel, nsp, ntp, layers),
        out_shape=jax.ShapeDtypeStruct((rows, size), half),
        in_specs=[anywhere] * 4 + [inside] + [anywhere] * 3,
        out_specs=anywhere,
        scratch_shapes=scratch,
        compiler_params=pltpu.CompilerParams(
            collective_id=0, has_side_effects=True, vmem_limit_bytes=VMEM_BYTES
        ),
        name="layers",
    )(stream_in, value_proj, gate_proj, out_proj, norm_gain, conv_taps, maps, forget_rate)


def solution(mesh):
    placed = (
        P("sp", "tp"),
        P(),
        P(None, "sp", "tp"),
        P(None, "sp", "tp"),
        P(None, "sp", "tp"),
        P(),
        P(None, None, None, "tp", None),
        P(),
    )
    return jax.shard_map(
        per_device, mesh=mesh, in_specs=placed, out_specs=P("sp", "tp"), check_vma=False
    )
```

profile of v0, /device:TPU:0, one launch (start us, length us, event | category | flops | bytes accessed | tf_op | source)
XLA Modules:
  0.0 491.3 jit_solution(15557117284986941819)
XLA Ops:
  0.0 489.1 %layers.1 = bf16[512,1024]{1,0:T(8,128)(2,1)} custom-call(bf16[512,1024]{1,0:T(8,128)(2,1)} %stream_ref.1, bf16[2,512,1024]{2,1,0:T(8,128)(2,1)} %value_ref.1, bf16[2,512,1024]{2,1,0:T(8,128)(2,1)} %gate_ref.1, bf16[2,512,1024]{2,1,0:T(8,128)(2,1)} %back_ref.1, f32[2,4096]{1,0:T(2,128)} %gain_ref.1, f32[2,4,4096]{2,1,0:T(4,128)} %taps_hbm.1, ...), custom_call_target="tpu_custom_call" | custom-call | tf_op jit(solution)/shard_map/layers/pallas_call | solution.py:627
  489.1 2.3 copy.10
where the time goes:
time: 492 us; the launch traced here: 491 us
  Pallas kernels  489 us (99%)
    pallas_call x1, Pallas kernels, per_device(): pl.pallas_call(functools.partial(kernel, nsp, ntp, layers), out_shape=jax...  489 us

commit v1 on v0

--- a/solution.py
+++ b/solution.py
@@ -45,7 +45,7 @@
     stream_ref, value_ref, gate_ref, back_ref, gain_ref, taps_hbm, gates_hbm, rate_hbm,
     result_ref,
     feats, weights, own, mix, gate_z, padded, fa, fu, ba, bu, fh, fp, bh, bp,
-    both, fcum, bcum, mixed, part, core_in, x_in, z_in, edges, ends, states, taps, gates, rate,
+    both, cums, mixed, part, core_in, x_in, z_in, edges, ends, states, taps, gates, rate,
     start_sem, own_sem, wz_send, wy_send, w_recv,
     fz_send, fz_recv, fx_send, fx_recv, fc_send, fc_recv,
     sz_send, sz_recv, sx_send, sx_recv, sc_send, sc_recv,
@@ -110,10 +110,9 @@
             w_recv.at[m, kz * ny + ky], y_peer(ky),
         )
 
-    def send_weights(ms):
-        for k in range(1, nz):
-            for m in ms:
-                z_weight(m, k).start()
+    def send_weights(*pairs):
+        for m, k in pairs:
+            z_weight(m, k).start()
 
     def send_own_weights(ms):
         for m in ms:
@@ -152,26 +151,28 @@
             src, slot, column, fx_send.at[slot, k - 1], fx_recv.at[slot, k - 1], x_peer(k)
         )
 
+    def f_to_z(src):
+        return f_copy(src, 1, column, fz_send.at[0], fz_recv.at[0], z_peer(1))
+
     def gather_start(src):
-        z_copy = f_copy(src, 1, column, fz_send.at[0], fz_recv.at[0], z_peer(1))
-        z_copy.start()
         for k in range(1, nx):
             f_to_x(0, k, src).start()
         f_to_core(0, 0, src).start()
 
-    def gather_rest():
-        f_copy(own, 1, column, fz_send.at[0], fz_recv.at[0], z_peer(1)).wait_recv()
+    def gather_z():
+        f_to_z(own).wait_recv()
         mine = feats.at[1, column]
         for k in range(1, nx):
             f_to_x(1, k, mine).start()
         f_to_core(1, 0, mine).start()
-        for slot in range(2):
-            for k in range(1, nx):
-                there = feats.at[slot, column_of(k)]
-                remote(
-                    own, there, fx_send.at[slot, k - 1], fx_recv.at[slot, k - 1], core_peer
-                ).wait_recv()
-                f_to_core(slot, k, there).start()
+
+    def gather_x(slot):
+        for k in range(1, nx):
+            there = feats.at[slot, column_of(k)]
+            remote(
+                own, there, fx_send.at[slot, k - 1], fx_recv.at[slot, k - 1], core_peer
+            ).wait_recv()
+            f_to_core(slot, k, there).start()
 
     def gather_finish(slot):
         for k in range(nx):
@@ -181,7 +182,7 @@
         for k in range(1, nx):
             f_to_x(slot, k, own).wait_send()
         if slot == 1:
-            f_copy(own, 1, column, fz_send.at[0], fz_recv.at[0], z_peer(1)).wait_send()
+            f_to_z(own).wait_send()
 
     def normalize(layer, slot):
         step = 16
@@ -201,48 +202,83 @@
                 feats[slot, t, at, :] = (values * scale * gain).astype(jnp.bfloat16)
             return 0
 
-        lax.fori_loop(0, rows // step, body, 0)
-
-    def owner_of(p):
-        kz, ky = div(p, ny), rem(p, ny)
+        lax.fori_loop(0, rows // step, body, 0, unroll=2)
+
+    def owner_of(kz, ky):
         return flip_bits(z, kz, nz) * ny + rem(y + ny - ky, ny)
 
-    def enter(layer, relayed):
-        fcum[...] = jnp.zeros_like(fcum)
-        bcum[...] = jnp.zeros_like(bcum)
-        first, second = 3 * layer, 3 * layer + 1
-
-        def body(p, _):
-            ky = rem(p, ny)
-            for m in (first, second):
-
-                @pl.when(ky != 0)
+    def table(j, values):
+        found = jnp.int32(values[0])
+        for i, value in enumerate(values):
+            found = jnp.where(j == i, jnp.int32(value), found)
+        return found
+
+    def nth(i):
+        return jnp.where(role == 1, jnp.int32(nz - 1 - i), jnp.int32(1 + i))
+
+    def all_steps(ms, order):
+        steps = [(m, kz, 0, None) for m in ms for kz in order]
+        return steps + [(m, kz, ky, None) for m in ms for kz in order for ky in range(1, ny)]
+
+    def late_steps(m):
+        order = [(0, 0)] + [(k, nz - k) for k in range(1, nz)]
+        steps = [(m, kz, 0, inner) for kz, inner in order]
+        return steps + [(m, kz, ky, inner) for kz, inner in order for ky in range(1, ny)]
+
+    def walk(steps, relays, waits, use, inner_relays=()):
+        steps = [(m, kz, ky, kz if inner is None else inner) for m, kz, ky, inner in steps]
+        columns = list(zip(*steps))
+        passing = [int(ky == 0 and kz != 0 and (m, kz) in relays) for m, kz, ky, _ in steps]
+        inside = [int(ky == 0 and kz != 0 and (m, kz) in inner_relays) for m, kz, ky, _ in steps]
+        waiting = [int(waits and ky != 0) for _, _, ky, _ in steps]
+
+        def body(j, _):
+            m, outer, ky, inner = [table(j, column) for column in columns]
+            kz = jnp.where(role == 1, inner, outer)
+
+            if any(passing):
+
+                @pl.when(table(j, passing) == 1)
                 def _():
-                    y_weight_wait(m, p)
-
-                if m not in relayed:
-
-                    @pl.when(jnp.logical_and(ky == 0, p != 0))
-                    def _():
-                        relay(m, div(p, ny))
-
-            owner = owner_of(p)
+                    relay(m, kz)
+
+            if any(waiting):
+
+                @pl.when(table(j, waiting) == 1)
+                def _():
+                    y_weight_wait(m, kz * ny + ky)
+
+            if any(inside):
+
+                @pl.when(jnp.logical_and(role == 1, table(j, inside) == 1))
+                def _():
+                    relay(m, kz)
+
+            use(m, kz, ky)
+            return 0
+
+        lax.fori_loop(0, len(steps), body, 0)
+
+    def clear(layer):
+        cums[...] = jnp.zeros_like(cums)
+        for m in (3 * layer, 3 * layer + 1):
+            own_weight(m).wait()
+
+    def enter(layer, slots, steps, relays, waits, inner_relays=()):
+        def use(m, kz, ky):
+            owner = owner_of(kz, ky)
             t = div(owner, per)
             at = pl.ds(pl.multiple_of(rem(owner, per) * depth, 128), depth)
-            for slot in range(2):
-                cells = feats[slot, t, :, at]
-                for m, total in ((first, fcum), (second, bcum)):
-                    total[slot] += jnp.dot(
-                        cells, weights[m, p], preferred_element_type=jnp.float32
-                    )
-            return 0
-
-        for m in (first, second):
-            own_weight(m).wait()
-        lax.fori_loop(0, nsp, body, 0)
-        for slot in range(2):
-            mix[slot] = fcum[slot].astype(jnp.bfloat16)
-            gate_z[slot] = bcum[slot].astype(jnp.bfloat16)
+            for slot in slots:
+                cums[m - 3 * layer, slot] += jnp.dot(
+                    feats[slot, t, :, at], weights[m, kz * ny + ky],
+                    preferred_element_type=jnp.float32,
+                )
+
+        walk(steps, relays, waits, use, inner_relays)
+        for slot in slots:
+            mix[slot] = cums[0, slot].astype(jnp.bfloat16)
+            gate_z[slot] = cums[1, slot].astype(jnp.bfloat16)
 
     def parity(slot):
         return rem(z + slot, 2)
@@ -255,29 +291,31 @@
         there = div(zb, 2) * ny + yb
         return rem(group + groups - there, groups), rem(zb, 2)
 
-    def exchange(cells, send, recv):
-        copies = [
+    def swaps(cells, send, recv):
+        return [
             remote(cells.at[0], cells.at[k], send.at[k - 1], recv.at[k - 1], group_peer(k))
             for k in range(1, groups)
         ]
-        for copy in copies:
-            copy.start()
-        for copy in copies:
-            copy.wait_recv()
-        for copy in copies:
-            copy.wait_send()
-
-    def exchange_edges():
+
+    def edges_begin():
         ends[0] = jnp.zeros(ends.shape[1:], jnp.float32)
         for slot in range(2):
             edges[0, parity(slot), 0:8, :] = mix[slot, rows - 8 : rows, :].astype(jnp.float32)
             edges[0, parity(slot), 8:16, :] = mix[slot, 0:8, :].astype(jnp.float32)
-        exchange(edges, edge_send, edge_recv)
+        for copy in swaps(edges, edge_send, edge_recv):
+            copy.start()
+
+    def edges_end():
+        for copy in swaps(edges, edge_send, edge_recv):
+            copy.wait_recv()
+        for copy in swaps(edges, edge_send, edge_recv):
+            copy.wait_send()
 
     def scan(layer, services):
         blocks = width // block
         chunk = rows // CHUNKS
         size = rows // ROW_STEPS
+        pitch = chunk + 8
 
         def body(i, _):
             for when, m, kz in services:
@@ -323,13 +361,17 @@
                     lost = fall * series
                     loss = lost * (2.0 - lost)
                     root = loss * lax.rsqrt(jnp.maximum(loss, 1e-30))
-                    decay_to[base : base + size, :] = 1.0 - lost
-                    drive_to[base : base + size, :] = root * sigmoid(pre_i) * conv
+                    decay = 1.0 - lost
+                    drive = root * sigmoid(pre_i) * conv
+                    for c in range(base // chunk, (base + size) // chunk):
+                        cut = slice(c * chunk - base, (c + 1) * chunk - base)
+                        decay_to[c * pitch : c * pitch + chunk, :] = decay[cut]
+                        drive_to[c * pitch : c * pitch + chunk, :] = drive[cut]
 
             def advance(j, carry):
                 f_state, f_prod, b_state, b_prod = carry
-                at = pl.ds(j, CHUNKS, stride=chunk)
-                back = pl.ds(chunk - 1 - j, CHUNKS, stride=chunk)
+                at = pl.ds(j, CHUNKS, stride=pitch)
+                back = pl.ds(chunk - 1 - j, CHUNKS, stride=pitch)
                 f_decay, b_decay = fa[at, :], ba[back, :]
                 f_state = f_decay * f_state + fu[at, :]
                 f_prod = f_decay * f_prod
@@ -363,18 +405,24 @@
             ends[0, even, 3:4, lanes] = state
             for c in range(CHUNKS):
                 at = slice(c * chunk, (c + 1) * chunk)
-                f_local, b_local = fp[at, :], bp[at, :]
+                held = slice(c * pitch, c * pitch + chunk)
+                f_local, b_local = fp[held, :], bp[held, :]
                 both[slot, at, lanes] = (
-                    fh[at, :] + f_local * f_in[c][0] + bh[at, :] + b_local * b_in[c][0]
+                    fh[held, :] + f_local * f_in[c][0] + bh[held, :] + b_local * b_in[c][0]
                 )
-                fcum[slot, at, lanes] = f_local * f_in[c][1]
-                bcum[slot, at, lanes] = b_local * b_in[c][1]
+                cums[0, slot, at, lanes] = f_local * f_in[c][1]
+                cums[1, slot, at, lanes] = b_local * b_in[c][1]
             return 0
 
         lax.fori_loop(0, 2 * blocks, body, 0)
 
     def exchange_ends():
-        exchange(ends, end_send, end_recv)
+        for copy in swaps(ends, end_send, end_recv):
+            copy.start()
+        for copy in swaps(ends, end_send, end_recv):
+            copy.wait_recv()
+        for copy in swaps(ends, end_send, end_recv):
+            copy.wait_send()
         for slot in range(2):
             where = token_block(slot)
             forward = jnp.zeros((1, width), jnp.float32)
@@ -390,42 +438,35 @@
             states[slot, 0:1, :] = forward
             states[slot, 1:2, :] = backward
 
-    def leave(layer, slot, first):
+    def leave(layer, slot, order, relays, waits):
         step = 32
         m = 3 * layer + 2
 
         def finish(i, _):
             at = pl.ds(pl.multiple_of(i * step, step), step)
-            total = both[slot, at, :] + fcum[slot, at, :] * states[slot, 0:1, :]
-            total = total + bcum[slot, at, :] * states[slot, 1:2, :]
+            total = both[slot, at, :] + cums[0, slot, at, :] * states[slot, 0:1, :]
+            total = total + cums[1, slot, at, :] * states[slot, 1:2, :]
             gate = gate_z[slot, at, :].astype(jnp.float32)
             mixed[at, :] = (total * gate * sigmoid(gate)).astype(jnp.bfloat16)
             return 0
 
         lax.fori_loop(0, rows // step, finish, 0)
 
-        def body(p, _):
-            if first:
-
-                @pl.when(rem(p, ny) != 0)
-                def _():
-                    y_weight_wait(m, p)
-
+        def use(_, kz, ky):
             term = lax.dot_general(
-                mixed[...], weights[m, p], (((1,), (1,)), ((), ())),
+                mixed[...], weights[m, kz * ny + ky], (((1,), (1,)), ((), ())),
                 preferred_element_type=jnp.float32,
             )
-            owner = owner_of(p)
+            owner = owner_of(kz, ky)
             t = div(owner, per)
             far = rem(div(t, 2) + nx - x, nx)
             other = rem(t + core, 2)
             at = pl.ds(pl.multiple_of(rem(owner, per) * depth, 128), depth)
             part[slot, other, far, :, at] = term.astype(jnp.bfloat16)
-            return 0
-
-        if first:
+
+        if waits:
             own_weight(m).wait()
-        lax.fori_loop(0, nsp, body, 0)
+        walk(all_steps((m,), order), relays, waits, use)
 
     def s_to_core(slot, k):
         return remote(
@@ -499,49 +540,105 @@
     first_own.start()
     first_feat.start()
     pl.semaphore_wait(barrier, len(peers))
+    order = [k for k in range(2, nz)] + [1]
+    far = order[:-1]
+    send_own_weights((0,))
+    send_weights((0, far[0]))
+    f_to_z(stream_ref).start()
     gather_start(stream_ref)
-    send_weights((0, 1))
-    send_own_weights((0, 1))
+    send_weights(*[(0, k) for k in far[1:]], (0, 1), (1, far[0]), (1, 1))
+    send_weights(*[(1, k) for k in far[1:]])
+    send_own_weights((1,))
     for m in range(3 * layers):
         own_weight(m).start()
     for copy in small:
         copy.start()
-    send_weights((2,))
+    send_weights(*[(2, k) for k in [far[0], 1] + far[1:]])
     send_own_weights((2,))
 
     for layer in range(layers):
         last = layer == layers - 1
-        gather_rest()
+        v, g, o = 3 * layer, 3 * layer + 1, 3 * layer + 2
+        clear(layer)
         if layer == 0:
+            gather_x(0)
+            relay(v, far[0])
+            gather_z()
             first_own.wait()
             first_feat.wait()
-        for slot in range(2):
-            gather_finish(slot)
-            normalize(layer, slot)
-        enter(layer, () if layer == 0 else (3 * layer,))
-        exchange_edges()
-        if not last:
-            send_weights((3 * layer + 3,))
-            send_own_weights((3 * layer + 3,))
+            gather_finish(0)
+            normalize(layer, 0)
+            for k in far[1:]:
+                relay(v, k)
+            gather_x(1)
+            relay(v, 1)
+            gather_finish(1)
+            normalize(layer, 1)
+            inward = [(v, kz, 0, None) for kz in [0] + order]
+            inward += [(g, kz, 0, None) for kz in [0, far[0], 1] + far[1:]]
+            inward += [
+                (m, kz, ky, None) for m in (v, g) for kz in [0] + order for ky in range(1, ny)
+            ]
+            passing = [(g, k) for k in order]
+            enter(layer, (0, 1), inward, passing, True)
+        else:
+            relay(g, nth(0))
+            gather_x(0)
+
+            @pl.when(role == 0)
+            def _():
+                for i in range(1, nz - 2):
+                    relay(g, nth(i))
+
+            gather_z()
+            gather_finish(0)
+            normalize(layer, 0)
+            inward = all_steps((v,), [0] + order) + late_steps(g)
+            middle = [(g, k) for k in range(2, nz - 1)]
+            enter(layer, (0,), inward, [(g, nz - 1)], True, middle)
+            relay(o, nth(0))
+            gather_x(1)
+            gather_finish(1)
+            for i in range(1, nz - 2):
+                relay(o, nth(i))
+            normalize(layer, 1)
+            enter(layer, (1,), inward, [], False)
+        edges_begin()
+        mixed_order = [far[0], 1] + far[1:]
+        if layer == 0:
+            for k in mixed_order:
+                relay(o, k)
+        edges_end()
         if layer == 0:
             for copy in small:
                 copy.wait()
-        blocks = 2 * (width // block)
-        services = [
-            (min(blocks - 1, (blocks * (k + 1)) // (nz + 1)), 3 * layer + 2, k)
-            for k in range(1, nz)
-        ]
-        scan(layer, services)
+        if not last:
+            send_weights((v + 3, 1))
+
+            @pl.when(role == 1)
+            def _():
+                send_weights((v + 4, 1))
+
+        scan(layer, [])
         exchange_ends()
-        leave(layer, 1, True)
+        if layer != 0:
+            relay(o, nth(nz - 2))
+        if not last:
+            send_weights(*[(v + 3, k) for k in far])
+
+            @pl.when(role == 1)
+            def _():
+                send_weights(*[(v + 4, k) for k in reversed(far)])
+
+            send_own_weights((v + 3, v + 4))
+        leave(layer, 1, [0] + order, [], True)
         give(1)
-        leave(layer, 0, False)
+        leave(layer, 0, [0] + order, [], False)
         pass_on(1)
         give(0)
         pass_on(0)
         if not last:
-            for k in range(1, nz):
-                relay(3 * layer + 3, k)
+            relay(v + 3, 1)
         land(1)
 
         def send_over(at):
@@ -549,7 +646,13 @@
 
         tiles(send_over)
         s_to_z().start()
+        if not last:
+            send_own_weights((v + 5,))
+            relay(v + 3, far[0])
         land(0)
+        if not last:
+            for k in far[1:]:
+                relay(v + 3, k)
         s_to_z().wait_recv()
 
         def renew(at):
@@ -561,9 +664,18 @@
 
         tiles(renew)
         if not last:
+            f_to_z(own).start()
             gather_start(own)
-            send_weights((3 * layer + 4, 3 * layer + 5))
-            send_own_weights((3 * layer + 4, 3 * layer + 5))
+
+            @pl.when(role == 0)
+            def _():
+                send_weights(*[(v + 4, k) for k in far], (v + 4, 1))
+                send_weights(*[(v + 5, k) for k in far], (v + 5, 1))
+
+            @pl.when(role == 1)
+            def _():
+                send_weights((v + 5, 1), *[(v + 5, k) for k in reversed(far)])
+
         drain(1)
         drain(0)
         s_to_z().wait_send()
@@ -591,7 +703,7 @@
     maps = block_gates.reshape(layers, 4, both_roles, block)
     half, full = jnp.bfloat16, jnp.float32
     dma = pltpu.SemaphoreType.DMA
-    slab = pltpu.VMEM((rows, block), full)
+    slab = pltpu.VMEM((rows + 8 * CHUNKS, block), full)
     scratch = [
         pltpu.VMEM((2, ntp, rows, size), half),
         pltpu.VMEM((3 * layers, nsp, depth, width), half),
@@ -600,7 +712,8 @@
         pltpu.VMEM((2, rows, width), half),
         pltpu.VMEM((rows + 16, block), full),
         *[slab] * 8,
-        *[pltpu.VMEM((2, rows, width), full)] * 3,
+        pltpu.VMEM((2, rows, width), full),
+        pltpu.VMEM((2, 2, rows, width), full),
         pltpu.VMEM((rows, width), half),
         pltpu.VMEM((2, 2, nx, rows, size), half),
         pltpu.VMEM((2, nx, rows, size), half),

time: 492 us -> 401 us (0.82)
  Pallas kernels: 489 us -> 399 us
    pallas_call x1, Pallas kernels: 489 us -> 399 us  [per_device(): pl.pallas_call(functools.partial(kernel, nsp, ntp, layers), out_shape=jax...]
where the time goes in v1:
time: 401 us
  Pallas kernels  399 us (100%)
    pallas_call x1, Pallas kernels, per_device(): pl.pallas_call(functools.partial(kernel, nsp, ntp, layers), out_shape=jax...  399 us

profile of v1, /device:TPU:0, one launch (start us, length us, event | category | flops | bytes accessed | tf_op | source)
XLA Modules:
  0.0 401.3 jit_solution(2289998149454586761)
XLA Ops:
  0.0 399.0 %layers.1 = bf16[512,1024]{1,0:T(8,128)(2,1)} custom-call(bf16[512,1024]{1,0:T(8,128)(2,1)} %stream_ref.1, bf16[2,512,1024]{2,1,0:T(8,128)(2,1)} %value_ref.1, bf16[2,512,1024]{2,1,0:T(8,128)(2,1)} %gate_ref.1, bf16[2,512,1024]{2,1,0:T(8,128)(2,1)} %back_ref.1, f32[2,4096]{1,0:T(2,128)} %gain_ref.1, f32[2,4,4096]{2,1,0:T(4,128)} %taps_hbm.1, ...), custom_call_target="tpu_custom_call" | custom-call | tf_op jit(solution)/shard_map/layers/pallas_call | solution.py:740
  399.0 2.3 copy.10

commit v2 on v1

--- a/solution.py
+++ b/solution.py
@@ -11,6 +11,7 @@
 NORM_EPS = 1e-06
 ROW_STEPS = 4
 CHUNKS = 8
+HALVES = 2
 MESH = pl.DeviceIdType.MESH
 VMEM_BYTES = 67043328
 SERIES = (1.0, -1.0 / 2, 1.0 / 6, -1.0 / 24, 1.0 / 120, -1.0 / 720, 1.0 / 5040)
@@ -135,60 +136,60 @@
             weights.at[m, p], weights.at[m, p], wz_send.at[m, 0], w_recv.at[m, p], core_peer
         ).wait_recv()
 
-    def f_copy(src, slot, at_column, send, recv, peer):
-        return remote(src, feats.at[slot, at_column], send, recv, peer)
+    split = rows // HALVES
+
+    def cut(h):
+        return pl.ds(h * split, split)
+
+    def f_copy(src, slot, h, at_column, send, recv, peer):
+        return remote(src.at[cut(h)], feats.at[slot, at_column, cut(h)], send, recv, peer)
 
     def column_of(k):
         return rem(x + nx - k, nx) * 2 + core
 
-    def f_to_core(slot, k, src):
+    def f_to_core(slot, k, h, src):
         return f_copy(
-            src, slot, column_of(k), fc_send.at[slot, k], fc_recv.at[slot, k], core_peer
+            src, slot, h, column_of(k), fc_send.at[slot, k, h], fc_recv.at[slot, k, h], core_peer
         )
 
-    def f_to_x(slot, k, src):
-        return f_copy(
-            src, slot, column, fx_send.at[slot, k - 1], fx_recv.at[slot, k - 1], x_peer(k)
-        )
-
-    def f_to_z(src):
-        return f_copy(src, 1, column, fz_send.at[0], fz_recv.at[0], z_peer(1))
-
-    def gather_start(src):
+    def f_to_x(slot, k, h, src):
+        send, recv = fx_send.at[slot, k - 1, h], fx_recv.at[slot, k - 1, h]
+        return f_copy(src, slot, h, column, send, recv, x_peer(k))
+
+    def f_to_z(h, src):
+        return f_copy(src, 1, h, column, fz_send.at[h], fz_recv.at[h], z_peer(1))
+
+    def gather_start(h, src):
         for k in range(1, nx):
-            f_to_x(0, k, src).start()
-        f_to_core(0, 0, src).start()
-
-    def gather_z():
-        f_to_z(own).wait_recv()
+            f_to_x(0, k, h, src).start()
+        f_to_core(0, 0, h, src).start()
+
+    def gather_z(h):
+        f_to_z(h, own).wait_recv()
         mine = feats.at[1, column]
         for k in range(1, nx):
-            f_to_x(1, k, mine).start()
-        f_to_core(1, 0, mine).start()
-
-    def gather_x(slot):
+            f_to_x(1, k, h, mine).start()
+        f_to_core(1, 0, h, mine).start()
+
+    def gather_x(slot, h):
         for k in range(1, nx):
-            there = feats.at[slot, column_of(k)]
-            remote(
-                own, there, fx_send.at[slot, k - 1], fx_recv.at[slot, k - 1], core_peer
-            ).wait_recv()
-            f_to_core(slot, k, there).start()
-
-    def gather_finish(slot):
+            f_to_x(slot, k, h, own).wait_recv()
+            f_to_core(slot, k, h, feats.at[slot, column_of(k)]).start()
+
+    def gather_finish(slot, h):
         for k in range(nx):
-            there = feats.at[slot, column_of(k)]
-            f_to_core(slot, k, there).wait_recv()
-            f_to_core(slot, k, there).wait_send()
+            f_to_core(slot, k, h, feats.at[slot, column_of(k)]).wait_recv()
+            f_to_core(slot, k, h, feats.at[slot, column_of(k)]).wait_send()
         for k in range(1, nx):
-            f_to_x(slot, k, own).wait_send()
+            f_to_x(slot, k, h, own).wait_send()
         if slot == 1:
-            f_to_z(own).wait_send()
-
-    def normalize(layer, slot):
+            f_to_z(h, own).wait_send()
+
+    def normalize(layer, slot, h):
         step = 16
 
         def body(i, _):
-            at = pl.ds(pl.multiple_of(i * step, step), step)
+            at = pl.ds(pl.multiple_of(h * split + i * step, step), step)
             squares = None
             for t in range(ntp):
                 values = feats[slot, t, at, :].astype(jnp.float32)
@@ -202,7 +203,7 @@
                 feats[slot, t, at, :] = (values * scale * gain).astype(jnp.bfloat16)
             return 0
 
-        lax.fori_loop(0, rows // step, body, 0, unroll=2)
+        lax.fori_loop(0, split // step, body, 0, unroll=2)
 
     def owner_of(kz, ky):
         return flip_bits(z, kz, nz) * ny + rem(y + ny - ky, ny)
@@ -416,9 +417,11 @@
 
         lax.fori_loop(0, 2 * blocks, body, 0)
 
-    def exchange_ends():
+    def ends_begin():
         for copy in swaps(ends, end_send, end_recv):
             copy.start()
+
+    def ends_end():
         for copy in swaps(ends, end_send, end_recv):
             copy.wait_recv()
         for copy in swaps(ends, end_send, end_recv):
@@ -468,46 +471,69 @@
             own_weight(m).wait()
         walk(all_steps((m,), order), relays, waits, use)
 
-    def s_to_core(slot, k):
+    def s_to_core(slot, k, h):
         return remote(
-            part.at[slot, 1, k], core_in.at[slot, k], sc_send.at[slot, k], sc_recv.at[slot, k],
-            core_peer,
+            part.at[slot, 1, k, cut(h)], core_in.at[slot, k, cut(h)],
+            sc_send.at[slot, k, h], sc_recv.at[slot, k, h], core_peer,
         )
 
-    def s_to_x(slot, k):
+    def s_to_x(slot, k, h):
         return remote(
-            part.at[slot, 0, k], x_in.at[slot, k - 1], sx_send.at[slot, k - 1],
-            sx_recv.at[slot, k - 1], x_peer(k),
+            part.at[slot, 0, k, cut(h)], x_in.at[slot, k - 1, cut(h)],
+            sx_send.at[slot, k - 1, h], sx_recv.at[slot, k - 1, h], x_peer(k),
         )
 
-    def s_to_z():
-        return remote(part.at[1, 0, 0], z_in, sz_send.at[0], sz_recv.at[0], z_peer(1))
+    def s_to_z(h, k=0):
+        there = z_in.at[cut(h)] if k == 0 else x_in.at[1, k - 1, cut(h)]
+        index = h if k == 0 else HALVES + k - 1
+        return remote(
+            part.at[1, 0, k, cut(h)], there, sz_send.at[index], sz_recv.at[index], z_peer(1)
+        )
 
     def give(slot):
+        for h in range(HALVES):
+            for k in list(range(1, nx)) + [0]:
+                s_to_core(slot, k, h).start()
+
+    def tiles(h, body):
+        step = 32
+
+        def run(i, _):
+            body(pl.ds(pl.multiple_of(h * split + i * step, step), step))
+            return 0
+
+        lax.fori_loop(0, split // step, run, 0)
+
+    def add_core(slot, k, h, more=None):
+        def body(at):
+            total = part[slot, 0, k, at, :].astype(jnp.float32)
+            total = total + core_in[slot, k, at, :].astype(jnp.float32)
+            if more is not None:
+                total = total + more[at, :].astype(jnp.float32)
+            part[slot, 0, k, at, :] = total.astype(jnp.bfloat16)
+
+        tiles(h, body)
+
+    def pass_on(slot, h):
+        for k in range(1, nx):
+            s_to_core(slot, k, h).wait_recv()
+            add_core(slot, k, h)
+            s_to_x(slot, k, h).start()
+        s_to_core(slot, 0, h).wait_recv()
+
+    def pass_over(h):
         for k in list(range(1, nx)) + [0]:
-            s_to_core(slot, k).start()
-
-    def tiles(body):
-        step = 32
-
-        def run(i, _):
-            body(pl.ds(pl.multiple_of(i * step, step), step))
-            return 0
-
-        lax.fori_loop(0, rows // step, run, 0)
-
-    def pass_on(slot):
+            s_to_core(1, k, h).wait_recv()
+            add_core(1, k, h)
+            s_to_z(h, k).start()
+
+    def pass_joined(h):
         for k in range(1, nx):
-            s_to_core(slot, k).wait_recv()
-
-            def body(at):
-                total = part[slot, 0, k, at, :].astype(jnp.float32)
-                total = total + core_in[slot, k, at, :].astype(jnp.float32)
-                part[slot, 0, k, at, :] = total.astype(jnp.bfloat16)
-
-            tiles(body)
-            s_to_x(slot, k).start()
-        s_to_core(slot, 0).wait_recv()
+            s_to_core(0, k, h).wait_recv()
+            s_to_z(h, k).wait_recv()
+            add_core(0, k, h, x_in.at[1, k - 1])
+            s_to_x(0, k, h).start()
+        s_to_core(0, 0, h).wait_recv()
 
     def summed(slot, at):
         total = part[slot, 0, 0, at, :].astype(jnp.float32)
@@ -516,15 +542,44 @@
             total = total + x_in[slot, k - 1, at, :].astype(jnp.float32)
         return total
 
-    def land(slot):
+    def land(slot, h):
         for k in range(1, nx):
-            s_to_x(slot, k).wait_recv()
-
-    def drain(slot):
-        for k in range(nx):
-            s_to_core(slot, k).wait_send()
-        for k in range(1, nx):
-            s_to_x(slot, k).wait_send()
+            s_to_x(slot, k, h).wait_recv()
+
+    def send_over(h):
+        land(1, h)
+
+        def body(at):
+            part[1, 0, 0, at, :] = summed(1, at).astype(jnp.bfloat16)
+
+        tiles(h, body)
+        s_to_z(h).start()
+
+    def renew(h, last):
+        land(0, h)
+        s_to_z(h).wait_recv()
+
+        def body(at):
+            total = summed(0, at) + z_in[at, :].astype(jnp.float32)
+            fresh = (own[at, :].astype(jnp.float32) + total).astype(jnp.bfloat16)
+            own[at, :] = fresh
+            if not last:
+                feats[0, column, at, :] = fresh
+
+        tiles(h, body)
+
+    def drain(crossed):
+        for h in range(HALVES):
+            for slot in range(2):
+                for k in range(nx):
+                    s_to_core(slot, k, h).wait_send()
+                for k in range(1, nx):
+                    if slot == 0 or h not in crossed:
+                        s_to_x(slot, k, h).wait_send()
+            s_to_z(h).wait_send()
+            for k in range(1, nx):
+                if h in crossed:
+                    s_to_z(h, k).wait_send()
 
     first_own = pltpu.make_async_copy(stream_ref, own, start_sem.at[0])
     first_feat = pltpu.make_async_copy(stream_ref, feats.at[0, column], start_sem.at[1])
@@ -542,72 +597,86 @@
     pl.semaphore_wait(barrier, len(peers))
     order = [k for k in range(2, nz)] + [1]
     far = order[:-1]
-    send_own_weights((0,))
+    halves = range(HALVES)
+    send_own_weights((0, 1))
     send_weights((0, far[0]))
-    f_to_z(stream_ref).start()
-    gather_start(stream_ref)
+    for h in halves:
+        f_to_z(h, stream_ref).start()
+        gather_start(h, stream_ref)
     send_weights(*[(0, k) for k in far[1:]], (0, 1), (1, far[0]), (1, 1))
-    send_weights(*[(1, k) for k in far[1:]])
-    send_own_weights((1,))
+    send_weights(*[(1, k) for k in far[1:]], (2, far[0]), (2, 1))
     for m in range(3 * layers):
         own_weight(m).start()
     for copy in small:
         copy.start()
-    send_weights(*[(2, k) for k in [far[0], 1] + far[1:]])
     send_own_weights((2,))
+    results = []
 
     for layer in range(layers):
         last = layer == layers - 1
         v, g, o = 3 * layer, 3 * layer + 1, 3 * layer + 2
         clear(layer)
         if layer == 0:
-            gather_x(0)
+            gather_x(0, 0)
             relay(v, far[0])
-            gather_z()
+            for h in range(1, HALVES):
+                gather_x(0, h)
+            for k in far[1:]:
+                relay(v, k)
+            for h in halves:
+                gather_z(h)
+            relay(v, 1)
             first_own.wait()
             first_feat.wait()
-            gather_finish(0)
-            normalize(layer, 0)
-            for k in far[1:]:
-                relay(v, k)
-            gather_x(1)
-            relay(v, 1)
-            gather_finish(1)
-            normalize(layer, 1)
-            inward = [(v, kz, 0, None) for kz in [0] + order]
-            inward += [(g, kz, 0, None) for kz in [0, far[0], 1] + far[1:]]
-            inward += [
-                (m, kz, ky, None) for m in (v, g) for kz in [0] + order for ky in range(1, ny)
-            ]
-            passing = [(g, k) for k in order]
-            enter(layer, (0, 1), inward, passing, True)
+            for h in halves:
+                gather_finish(0, h)
+                normalize(layer, 0, h)
+            relay(g, far[0])
+            for h in halves:
+                gather_x(1, h)
+            relay(g, 1)
+            for h in halves:
+                gather_finish(1, h)
+                normalize(layer, 1, h)
+            inward = all_steps((v,), [0] + order)
+            inward += all_steps((g,), [0, far[0], 1] + far[1:])
+            enter(layer, (0, 1), inward, [(g, k) for k in far[1:]], True)
         else:
             relay(g, nth(0))
-            gather_x(0)
+            for h in halves:
+                gather_x(0, h)
+                gather_z(h)
 
             @pl.when(role == 0)
             def _():
                 for i in range(1, nz - 2):
                     relay(g, nth(i))
 
-            gather_z()
-            gather_finish(0)
-            normalize(layer, 0)
+            @pl.when(role == 1)
+            def _():
+                send_weights((o, 1), *[(o, k) for k in reversed(far)])
+
+            for h in halves:
+                gather_finish(0, h)
+                normalize(layer, 0, h)
             inward = all_steps((v,), [0] + order) + late_steps(g)
             middle = [(g, k) for k in range(2, nz - 1)]
             enter(layer, (0,), inward, [(g, nz - 1)], True, middle)
             relay(o, nth(0))
-            gather_x(1)
-            gather_finish(1)
+            for h in halves:
+                gather_x(1, h)
+            for h in halves:
+                gather_finish(1, h)
+                normalize(layer, 1, h)
+            enter(layer, (1,), inward, [], False)
+        edges_begin()
+        if layer == 0:
+            send_weights(*[(o, k) for k in far[1:]])
+            relay(o, far[0])
+            relay(o, 1)
+        else:
             for i in range(1, nz - 2):
                 relay(o, nth(i))
-            normalize(layer, 1)
-            enter(layer, (1,), inward, [], False)
-        edges_begin()
-        mixed_order = [far[0], 1] + far[1:]
-        if layer == 0:
-            for k in mixed_order:
-                relay(o, k)
         edges_end()
         if layer == 0:
             for copy in small:
@@ -620,7 +689,11 @@
                 send_weights((v + 4, 1))
 
         scan(layer, [])
-        exchange_ends()
+        ends_begin()
+        if layer == 0:
+            for k in far[1:]:
+                relay(o, k)
+        ends_end()
         if layer != 0:
             relay(o, nth(nz - 2))
         if not last:
@@ -633,61 +706,61 @@
             send_own_weights((v + 3, v + 4))
         leave(layer, 1, [0] + order, [], True)
         give(1)
+        crossed = [h for h in halves if last and h >= (HALVES + 1) // 2]
+        for h in halves:
+            if h in crossed:
+                pass_over(h)
+            else:
+                pass_on(1, h)
         leave(layer, 0, [0] + order, [], False)
-        pass_on(1)
         give(0)
-        pass_on(0)
+        for h in halves:
+            if h in crossed:
+                pass_joined(h)
+            else:
+                pass_on(0, h)
         if not last:
             relay(v + 3, 1)
-        land(1)
-
-        def send_over(at):
-            part[1, 0, 0, at, :] = summed(1, at).astype(jnp.bfloat16)
-
-        tiles(send_over)
-        s_to_z().start()
+        for h in halves:
+            if h not in crossed:
+                send_over(h)
         if not last:
+
+            @pl.when(role == 0)
+            def _():
+                send_weights((v + 4, far[0]))
+
             send_own_weights((v + 5,))
             relay(v + 3, far[0])
-        land(0)
+        for h in halves:
+            renew(h, last)
+            if not last:
+                f_to_z(h, own).start()
+                gather_start(h, own)
+            else:
+                result = pltpu.make_async_copy(
+                    own.at[cut(h)], result_ref.at[cut(h)], out_sem.at[h]
+                )
+                result.start()
+                results.append(result)
         if not last:
             for k in far[1:]:
                 relay(v + 3, k)
-        s_to_z().wait_recv()
-
-        def renew(at):
-            total = summed(0, at) + z_in[at, :].astype(jnp.float32)
-            fresh = (own[at, :].astype(jnp.float32) + total).astype(jnp.bfloat16)
-            own[at, :] = fresh
-            if not last:
-                feats[0, column, at, :] = fresh
-
-        tiles(renew)
-        if not last:
-            f_to_z(own).start()
-            gather_start(own)
 
             @pl.when(role == 0)
             def _():
-                send_weights(*[(v + 4, k) for k in far], (v + 4, 1))
+                send_weights(*[(v + 4, k) for k in far[1:]], (v + 4, 1))
                 send_weights(*[(v + 5, k) for k in far], (v + 5, 1))
 
-            @pl.when(role == 1)
-            def _():
-                send_weights((v + 5, 1), *[(v + 5, k) for k in reversed(far)])
-
-        drain(1)
-        drain(0)
-        s_to_z().wait_send()
-    result = pltpu.make_async_copy(own, result_ref, out_sem.at[0])
-    result.start()
+        drain(crossed)
     for m in range(3 * layers):
         for k in range(1, nz):
             z_weight(m, k).wait_send()
         for kz in range(nz):
             for ky in range(1, ny):
                 y_weight(m, kz, ky, kz == 0).wait_send()
-    result.wait()
+    for result in results:
+        result.wait()
 
 
 def per_device(
@@ -730,10 +803,12 @@
         dma((3 * layers, nz - 1)),
         dma((3 * layers, nz, ny - 1)),
         dma((3 * layers, nsp)),
-        dma((1,)), dma((1,)), dma((2, nx - 1)), dma((2, nx - 1)), dma((2, nx)), dma((2, nx)),
-        dma((1,)), dma((1,)), dma((2, nx - 1)), dma((2, nx - 1)), dma((2, nx)), dma((2, nx)),
+        dma((HALVES,)), dma((HALVES,)),
+        *[dma((2, nx - 1, HALVES))] * 2, *[dma((2, nx, HALVES))] * 2,
+        dma((HALVES + nx - 1,)), dma((HALVES + nx - 1,)),
+        *[dma((2, nx - 1, HALVES))] * 2, *[dma((2, nx, HALVES))] * 2,
         dma((groups - 1,)), dma((groups - 1,)), dma((groups - 1,)), dma((groups - 1,)),
-        dma((1,)),
+        dma((HALVES,)),
     ]
     anywhere = pl.BlockSpec(memory_space=pl.ANY)
     inside = pl.BlockSpec(memory_space=pltpu.VMEM)

time: 401 us -> 386 us (0.963)
  Pallas kernels: 399 us -> 383 us
    pallas_call x1, Pallas kernels: 399 us -> 383 us  [per_device(): pl.pallas_call(functools.partial(kernel, nsp, ntp, layers), out_shape=jax...]
where the time goes in v2:
time: 386 us; the launch traced here: 385 us
  Pallas kernels  383 us (99%)
    pallas_call x1, Pallas kernels, per_device(): pl.pallas_call(functools.partial(kernel, nsp, ntp, layers), out_shape=jax...  383 us

profile of v2, /device:TPU:0, one launch (start us, length us, event | category | flops | bytes accessed | tf_op | source)
XLA Modules:
  0.0 385.1 jit_solution(15868887819892428527)
XLA Ops:
  0.0 382.9 %layers.1 = bf16[512,1024]{1,0:T(8,128)(2,1)} custom-call(bf16[512,1024]{1,0:T(8,128)(2,1)} %stream_ref.1, bf16[2,512,1024]{2,1,0:T(8,128)(2,1)} %value_ref.1, bf16[2,512,1024]{2,1,0:T(8,128)(2,1)} %gate_ref.1, bf16[2,512,1024]{2,1,0:T(8,128)(2,1)} %back_ref.1, f32[2,4096]{1,0:T(2,128)} %gain_ref.1, f32[2,4,4096]{2,1,0:T(4,128)} %taps_hbm.1, ...), custom_call_target="tpu_custom_call" | custom-call | tf_op jit(solution)/shard_map/layers/pallas_call | solution.py:815
  382.9 2.3 copy.10

commit v3 on v2

--- a/solution.py
+++ b/solution.py
@@ -11,7 +11,7 @@
 NORM_EPS = 1e-06
 ROW_STEPS = 4
 CHUNKS = 8
-HALVES = 2
+HALVES = 4
 MESH = pl.DeviceIdType.MESH
 VMEM_BYTES = 67043328
 SERIES = (1.0, -1.0 / 2, 1.0 / 6, -1.0 / 24, 1.0 / 120, -1.0 / 720, 1.0 / 5040)
@@ -485,7 +485,7 @@
 
     def s_to_z(h, k=0):
         there = z_in.at[cut(h)] if k == 0 else x_in.at[1, k - 1, cut(h)]
-        index = h if k == 0 else HALVES + k - 1
+        index = k * HALVES + h
         return remote(
             part.at[1, 0, k, cut(h)], there, sz_send.at[index], sz_recv.at[index], z_peer(1)
         )
@@ -693,9 +693,9 @@
         if layer == 0:
             for k in far[1:]:
                 relay(o, k)
+        else:
+            relay(o, nth(nz - 2))
         ends_end()
-        if layer != 0:
-            relay(o, nth(nz - 2))
         if not last:
             send_weights(*[(v + 3, k) for k in far])
 
@@ -805,7 +805,7 @@
         dma((3 * layers, nsp)),
         dma((HALVES,)), dma((HALVES,)),
         *[dma((2, nx - 1, HALVES))] * 2, *[dma((2, nx, HALVES))] * 2,
-        dma((HALVES + nx - 1,)), dma((HALVES + nx - 1,)),
+        dma((nx * HALVES,)), dma((nx * HALVES,)),
         *[dma((2, nx - 1, HALVES))] * 2, *[dma((2, nx, HALVES))] * 2,
         dma((groups - 1,)), dma((groups - 1,)), dma((groups - 1,)), dma((groups - 1,)),
         dma((HALVES,)),

time: 386 us -> 384 us (level)
  no operation moved by 1% of the time
where the time goes in v3:
time: 384 us
  Pallas kernels  382 us (99%)
    pallas_call x1, Pallas kernels, per_device(): pl.pallas_call(functools.partial(kernel, nsp, ntp, layers), out_shape=jax...  382 us

profile of v3, /device:TPU:0, one launch (start us, length us, event | category | flops | bytes accessed | tf_op | source)
XLA Modules:
  0.0 384.2 jit_solution(7619587736864091968)
XLA Ops:
  0.0 381.9 %layers.1 = bf16[512,1024]{1,0:T(8,128)(2,1)} custom-call(bf16[512,1024]{1,0:T(8,128)(2,1)} %stream_ref.1, bf16[2,512,1024]{2,1,0:T(8,128)(2,1)} %value_ref.1, bf16[2,512,1024]{2,1,0:T(8,128)(2,1)} %gate_ref.1, bf16[2,512,1024]{2,1,0:T(8,128)(2,1)} %back_ref.1, f32[2,4096]{1,0:T(2,128)} %gain_ref.1, f32[2,4,4096]{2,1,0:T(4,128)} %taps_hbm.1, ...), custom_call_target="tpu_custom_call" | custom-call | tf_op jit(solution)/shard_map/layers/pallas_call | solution.py:815
  381.9 2.3 copy.10
